TPU v7x, 32 devices: a whole 2x2x4 slice. The times are simulated.
32 devices in a mesh: grp: 2 (over y), fs: 8 (over z, core), tp: 2 (over x).
Axes of the slice: x: 2, y: 2, z: 4, core: 2. Of those that a mesh axis runs over, the one named last changes fastest.
Arguments:
- prompt: bfloat16 [6144, 2048], P(('grp', 'fs')), parts along dimension 0, may hold values from -6 to 6
- routes: int32 [6144, 4], P(('grp', 'fs')), parts along dimension 0, may hold values from 0 to 7, all different within a row; in each aligned block of 384 rows (0 to 383, 384 to 767, ...) at most 240 rows name the same one
- route_weight: float32 [6144, 4], P(('grp', 'fs')), parts along dimension 0, may hold values from 0.2 to 1
- norm_gain: float32 [2048], P('fs'), may hold values from 0.1 to 1.9
- gate_train: float32 [8, 2048, 1024], P(None, 'fs', 'tp'), may hold values from -0.4 to 0.4
- up_train: float32 [8, 2048, 1024], P(None, 'fs', 'tp'), may hold values from -0.4 to 0.4
- down_train: float32 [8, 1024, 2048], P(None, 'fs', 'tp'), may hold values from -0.07 to 0.07
Outputs:
- gate_serve: bfloat16 [16, 2048, 1024], P(('grp', 'fs'), None, 'tp'), parts along dimension 0
- up_serve: bfloat16 [16, 2048, 1024], P(('grp', 'fs'), None, 'tp'), parts along dimension 0
- down_serve: bfloat16 [16, 1024, 2048], P(('grp', 'fs'), 'tp'), parts along dimension 0
- mixed: bfloat16 [6144, 2048], P(('grp', 'fs'), 'tp'), parts along dimension 0
There are 2 independent parts, one for each index of `grp`. A program takes and returns all parts, laid end to end along the dimension named above; an argument that names none is the same for every part. Nothing has to cross between parts.
Inputs may be any that keep to these rules, and one draw needn't show every extreme that they name: `routes`: each row names 4 different experts. Among the rows of one index of fs no expert is named more than 240 times, a bound that some block reaches on some index.
All inputs are finite; a program needn't handle non-finite values.
Results may differ from a plain program's by a relative error of at most 0.012.
Values may be sent and summed in bfloat16 or wider, within the bound.
No kernel may reach another device: no remote copies, remote signals or barrier semaphores. Data moves between devices by JAX's collectives and lax.ppermute only.
A program may use at most 128 MiB of HBM per device.

v0:
```python
import jax
import jax.numpy as jnp
from jax import lax
from jax.sharding import PartitionSpec as P

TOP = 4
LIMIT = 7.0
ALPHA = 1.702
EPS = 1e-06


def shards(prompt, routes, route_weight, norm_gain, gate_train, up_train, down_train):
    gate_cast = (norm_gain[None, :, None] * gate_train).astype(jnp.bfloat16)
    up_cast = (norm_gain[None, :, None] * up_train).astype(jnp.bfloat16)
    down_cast = down_train.astype(jnp.bfloat16)
    gate_mine, up_mine = (
        lax.all_to_all(gate_cast, "fs", split_axis=0, concat_axis=1, tiled=True),
        lax.all_to_all(up_cast, "fs", split_axis=0, concat_axis=1, tiled=True),
    )
    down_rows = lax.all_to_all(down_cast, "fs", split_axis=0, concat_axis=1, tiled=True)
    down_mine = lax.all_to_all(down_rows, "tp", split_axis=1, concat_axis=2, tiled=True)
    tok_rows, width = prompt.shape
    experts = gate_train.shape[0]
    quarter = width // lax.axis_size("tp")
    capacity = min(tok_rows, max(2, 5 * tok_rows * TOP // (4 * experts)))
    values = prompt.astype(jnp.float32)
    normed = (values * lax.rsqrt(jnp.mean(values * values, axis=-1, keepdims=True) + EPS)).astype(
        jnp.bfloat16
    )
    flat_expert = routes.reshape(-1)
    onehot = (flat_expert[:, None] == jnp.arange(experts, dtype=jnp.int32)[None, :]).astype(
        jnp.int32
    )
    earlier = jnp.cumsum(onehot, axis=0) - onehot
    slot_pos = jnp.sum(earlier * onehot, axis=1)
    target = flat_expert * capacity + slot_pos
    source_row = jnp.arange(tok_rows * TOP, dtype=jnp.int32) // TOP
    outbox = jnp.zeros((experts * capacity, width), jnp.bfloat16).at[target].set(normed[source_row])
    inbox = lax.all_to_all(
        outbox.reshape(experts, capacity, width), "fs", split_axis=0, concat_axis=1, tiled=True
    )
    gate_pre = jnp.einsum("erd,edf->erf", inbox, gate_mine, preferred_element_type=jnp.float32)
    up_pre = jnp.einsum("erd,edf->erf", inbox, up_mine, preferred_element_type=jnp.float32)
    gate_pre = jnp.minimum(gate_pre, LIMIT)
    up_pre = jnp.clip(up_pre, -LIMIT, LIMIT)
    hidden = ((up_pre + 1.0) * gate_pre * jax.nn.sigmoid(ALPHA * gate_pre)).astype(jnp.bfloat16)
    own_width = hidden.shape[2]
    empty = jnp.zeros((hidden.shape[0], hidden.shape[1], down_rows.shape[2]), jnp.float32)
    total = empty
    piece = lax.all_gather(hidden, "tp", axis=2, tiled=True)
    for index in range(piece.shape[2] // own_width):
        cols = piece[:, :, index * own_width : (index + 1) * own_width]
        weight_rows = lax.dynamic_slice_in_dim(down_rows, index * own_width, own_width, 1)
        part = jnp.einsum(
            "erf,efd->erd", cols, weight_rows, preferred_element_type=jnp.float32
        ).astype(jnp.bfloat16)
        total = total + part.astype(jnp.float32)
    summed = total.astype(jnp.bfloat16)
    back = lax.all_to_all(summed, "fs", split_axis=1, concat_axis=0, tiled=True)
    picked = back.reshape(experts * capacity, quarter)[target].astype(jnp.float32)
    weighted = picked.reshape(tok_rows, TOP, quarter) * route_weight[:, :, None]
    mixed = jnp.sum(weighted, axis=1).astype(jnp.bfloat16)
    return (gate_mine, up_mine, down_mine, mixed)


def solution(mesh):
    return jax.shard_map(
        shards,
        mesh=mesh,
        in_specs=(
            P(("grp", "fs"), None),
            P(("grp", "fs"), None),
            P(("grp", "fs"), None),
            P("fs"),
            P(None, "fs", "tp"),
            P(None, "fs", "tp"),
            P(None, "fs", "tp"),
        ),
        out_specs=(
            P(("grp", "fs"), None, "tp"),
            P(("grp", "fs"), None, "tp"),
            P(("grp", "fs"), "tp", None),
            P(("grp", "fs"), "tp"),
        ),
        check_vma=False,
    )
```

profile of v0, /device:TPU:0, one launch (start us, length us, event | category | flops | bytes accessed | tf_op | source)
XLA Modules:
  0.0 601.2 jit_solution(9907944391653193153)
XLA Ops:
  7.2 6.8 %multiply_convert_fusion = (bf16[8,256,512]{2,1,0:T(8,128)(2,1)}, bf16[8,256,512]{2,1,0:T(8,128)(2,1)}) fusion(f32[8,256,512]{2,1,0:T(8,128)} %param.12, f32[256]{0:T(256)} %param.10, f32[8,256,512]{2,1,0:T(8,128)} %param.11), kind=kLoop, calls=%fused_computation.7 | loop fusion | flops 4194304 | bytes 12583936 | tf_op jit(solution)/shard_map/convert_element_type | solution.py:14
  14.0 6.5 %all-to-all-start = ((bf16[8,256,512]{2,1,0:T(8,128)(2,1)}), bf16[8,256,512]{2,1,0:T(8,128)(2,1)S(1)}, u32[]{:S(2)}, u32[]{:S(2)}) async-start(bf16[8,256,512]{2,1,0:T(8,128)(2,1)} %get-tuple-element.17), calls=%async_computation | async-start | bytes 4194304 | tf_op jit(solution)/shard_map/all_to_all | solution.py:17
  26.5 2.9 fusion.5
  29.4 33.0 %scatter_custom_fusion = bf16[1920,2048]{1,0:T(8,128)(2,1)} fusion(s32[1536]{0:T(1024)S(1)} %fusion.11, bf16[384,2048]{1,0:T(8,128)(2,1)} %fusion.5, s32[2048]{0:T(1024)S(1)} %pad_clamp_fusion.1, bf16[]{:T(256)} %constant.17.clone.1), kind=kCustom, calls=%fused_computation.4 | custom fusion | bytes 7864832 | tf_op jit(solution)/shard_map/scatter | solution.py:38
  62.4 7.1 %all-to-all-done = bf16[8,256,512]{2,1,0:T(8,128)(2,1)S(1)} async-done(((bf16[8,256,512]{2,1,0:T(8,128)(2,1)}), bf16[8,256,512]{2,1,0:T(8,128)(2,1)S(1)}, u32[]{:S(2)}, u32[]{:S(2)}) %all-to-all-start) | async-done | bytes 2097184 | tf_op jit(solution)/shard_map/all_to_all | solution.py:17
  69.5 178.2 %all_to_all.72 = bf16[8,240,2048]{2,1,0:T(8,128)(2,1)} all-to-all(bf16[8,240,2048]{2,1,0:T(8,128)(2,1)} %bitcast.61), channel_id=1, replica_groups=mesh['grp'=2,'fs'=8,'tp'=2] {'fs'}, dimensions={0} | all-to-all | bytes 15728640 | tf_op jit(solution)/shard_map/all_to_all | solution.py:39
  247.7 4.4 all-to-all-start.1
  252.1 9.5 %fusion.13 = f32[1920,512]{1,0:T(8,128)} fusion(bf16[1920,2048]{1,0:T(8,128)(2,1)} %bitcast.73, bf16[2048,512]{1,0:T(8,128)(2,1)S(1)} %bitcast.70), kind=kOutput, calls=%fused_computation.45 | convolution fusion | flops 4026531840 | bytes 13893632 | tf_op jit(solution)/shard_map/erd,edf->erf/dot_general | solution.py:42
  261.6 39.5 %all-to-all-done.1 = bf16[8,256,512]{2,1,0:T(8,128)(2,1)} async-done(((bf16[8,256,512]{2,1,0:T(8,128)(2,1)}), bf16[8,256,512]{2,1,0:T(8,128)(2,1)}, u32[]{:S(2)}, u32[]{:S(2)}) %all-to-all-start.1) | async-done | bytes 2097184 | tf_op jit(solution)/shard_map/all_to_all | solution.py:18
  301.1 11.8 %multiply_convert_fusion.2 = bf16[1920,512]{1,0:T(8,128)(2,1)} fusion(f32[1920,512]{1,0:T(8,128)} %fusion.13, bf16[1920,2048]{1,0:T(8,128)(2,1)} %bitcast.74, bf16[2048,512]{1,0:T(8,128)(2,1)} %bitcast.8), kind=kOutput, calls=%fused_computation.11 | convolution fusion | flops 4036362240 | bytes 15859712 | tf_op jit(solution)/shard_map/erd,edf->erf/dot_general | solution.py:43
  312.9 2.5 convert_element_type.62
  315.4 51.7 %all_to_all.73 = bf16[8,128,1024]{2,1,0:T(8,128)(2,1)S(1)} all-to-all(bf16[8,128,1024]{2,1,0:T(8,128)(2,1)S(1)} %convert_element_type.62), channel_id=1, replica_groups=mesh['grp'=2,'fs'=8,'tp'=2] {'fs'}, dimensions={0} | all-to-all | bytes 4194304 | tf_op jit(solution)/shard_map/all_to_all | solution.py:20
  368.4 5.2 copy.46
  374.1 12.8 %reduce.6 = bf16[1024,1024]{1,0:T(8,128)(2,1)S(1)} reduce(bf16[1024,1,1024]{2,1,0:T(2,128)(2,1)} %bitcast.64, bf16[]{:T(256)} %broadcast.146), dimensions={1}, to_apply=%bitcast.58.reduce_sub_computation | reduce | bytes 4194306
  386.9 2.5 reshape.227
  389.4 4.2 all-to-all-start.3
  393.6 4.2 fusion.6
  400.1 27.0 %copy.45 = bf16[1,1920,1024]{2,0,1:T(2,128)(2,1)} copy(bf16[1,1920,1024]{2,1,0:T(8,128)(2,1)S(1)} %fusion.2) | data formatting | bytes 7864320 | tf_op jit(solution)/shard_map/convert_element_type | solution.py:58
  427.1 24.6 %reduce.7 = bf16[1920,1024]{1,0:T(8,128)(2,1)} reduce(bf16[1920,1,1024]{2,1,0:T(2,128)(2,1)} %bitcast.62, bf16[]{:T(256)} %broadcast.146), dimensions={1}, to_apply=%bitcast.57.reduce_sub_computation | reduce | bytes 7864322
  451.7 7.6 %reshape.225 = bf16[8,2,122880]{2,1,0:T(2,128)(2,1)} reshape(bf16[1920,1024]{1,0:T(8,128)(2,1)} %reduce.7) | data formatting | bytes 7864320
  459.3 4.8 all-to-all-start.5
  464.3 3.1 reshape.228
  467.4 3.0 copy.37
  470.4 2.6 copy.30
  473.0 3.9 copy.36
  476.9 75.6 %all-to-all-done.5 = bf16[8,2,122880]{2,1,0:T(2,128)(2,1)} async-done(((bf16[8,2,122880]{2,1,0:T(2,128)(2,1)}), bf16[8,2,122880]{2,1,0:T(2,128)(2,1)}, u32[]{:S(2)}, u32[]{:S(2)}) %all-to-all-start.5) | async-done | bytes 3932192 | tf_op jit(solution)/shard_map/all_to_all | solution.py:59
  552.5 8.5 %reshape.226 = bf16[1920,1,1024]{2,1,0:T(2,128)(2,1)} reshape(bf16[8,2,122880]{2,1,0:T(2,128)(2,1)} %all-to-all-done.5) | data formatting | bytes 7864320
  561.0 6.8 %copy.44 = bf16[1,1920,1024]{2,1,0:T(8,128)(2,1)} copy(bf16[1,1920,1024]{2,0,1:T(2,128)(2,1)} %bitcast.63) | data formatting | bytes 7864320
  567.8 9.7 %gather_fusion = bf16[1536,1024]{1,0:T(8,128)(2,1)S(1)} fusion(bf16[1920,1024]{1,0:T(8,128)(2,1)} %bitcast.60, s32[2048]{0:T(1024)S(1)} %pad_clamp_fusion), kind=kCustom, calls=%fused_computation.1 | custom fusion | bytes 6297600 | tf_op jit(solution)/shard_map/gather | solution.py:60
  577.5 4.4 reshape.190
  581.9 7.9 %multiply_reduce_fusion = bf16[384,1024]{1,0:T(8,128)(2,1)} fusion(f32[384,4,1024]{2,1,0:T(4,128)} %reshape.190, f32[384,4]{1,0:T(8,128)S(1)} %copy.35), kind=kLoop, calls=%fused_computation.6 | loop fusion | flops 2752512 | bytes 7084032 | tf_op jit(solution)/shard_map/reduce_sum | solution.py:62
  591.1 3.0 copy.50
  (40 shorter events, 11.7 us)
Async XLA Ops:
  14.0 6.5 %copy-start.4 = (s32[384,4]{0,1:T(4,128)S(1)}, s32[384,4]{0,1:T(4,128)}, u32[]{:S(2)}) copy-start(s32[384,4]{0,1:T(4,128)} %param.8) | copy-start | bytes 18436
  14.0 55.5 %all-to-all-start = ((bf16[8,256,512]{2,1,0:T(8,128)(2,1)}), bf16[8,256,512]{2,1,0:T(8,128)(2,1)S(1)}, u32[]{:S(2)}, u32[]{:S(2)}) async-start(bf16[8,256,512]{2,1,0:T(8,128)(2,1)} %get-tuple-element.17), calls=%async_computation | async-start | bytes 4194304 | tf_op jit(solution)/shard_map/all_to_all | solution.py:17
  69.5 182.6 %copy-start.2 = (bf16[8,256,512]{2,1,0:T(8,128)(2,1)}, bf16[8,256,512]{2,1,0:T(8,128)(2,1)S(1)}, u32[]{:S(2)}) copy-start(bf16[8,256,512]{2,1,0:T(8,128)(2,1)S(1)} %all-to-all-done) | copy-start | bytes 6291460
  247.7 53.4 %all-to-all-start.1 = ((bf16[8,256,512]{2,1,0:T(8,128)(2,1)}), bf16[8,256,512]{2,1,0:T(8,128)(2,1)}, u32[]{:S(2)}, u32[]{:S(2)}) async-start(bf16[8,256,512]{2,1,0:T(8,128)(2,1)} %get-tuple-element.16), calls=%async_computation.1 | async-start | bytes 4194304 | tf_op jit(solution)/shard_map/all_to_all | solution.py:18
  252.1 141.5 %all-gather.3.cloned.1.call-start = ((), (), s32[]{:S(2)}) async-start(), calls=%async_computation.6 | async-start | bytes 5898240 | tf_op jit(solution)/shard_map/all_gather | solution.py:50
  367.1 1.3 copy-start
  389.4 69.9 %all-to-all-start.3 = ((bf16[2,2,262144]{2,1,0:T(2,128)(2,1)}), bf16[2,2,262144]{2,1,0:T(2,128)(2,1)S(1)}, u32[]{:S(2)}, u32[]{:S(2)}) async-start(bf16[2,2,262144]{2,1,0:T(2,128)(2,1)} %reshape.227), calls=%async_computation.3 | async-start | bytes 4194304 | tf_op jit(solution)/shard_map/all_to_all | solution.py:21
  393.6 4.2 copy-start.1
  393.6 4.2 copy-start.6
  459.3 4.9 copy-start.5
  459.3 93.2 %all-to-all-start.5 = ((bf16[8,2,122880]{2,1,0:T(2,128)(2,1)}), bf16[8,2,122880]{2,1,0:T(2,128)(2,1)}, u32[]{:S(2)}, u32[]{:S(2)}) async-start(bf16[8,2,122880]{2,1,0:T(2,128)(2,1)} %reshape.225), calls=%async_computation.5 | async-start | bytes 7864320 | tf_op jit(solution)/shard_map/all_to_all | solution.py:59
  581.9 7.9 %copy-start.3 = (bf16[8,256,512]{2,1,0:T(8,128)(2,1)S(1)}, bf16[8,256,512]{2,1,0:T(8,128)(2,1)}, u32[]{:S(2)}) copy-start(bf16[8,256,512]{2,1,0:T(8,128)(2,1)} %copy-done.2) | copy-start | bytes 6291460
Sparse Core Ops, SparseCore 0:
  313.0 52.6 all-gather.2
where the time goes:
time: 605 us; the launch traced here: 601 us
  blocking collectives  230 us (38%)
  local copies, waits for them, and re-layouts  125 us (21%)
  waiting for transfers between devices  122 us (20%)
  other arithmetic  62.4 us (10%)
  matrix products  27.7 us (5%)
  starting transfers between devices  19.9 us (3%)
  between operations  14.4 us (2%)
    all_to_all x1, blocking collectives, shards(): lax.all_to_all(outbox.reshape(experts, capacity, width), 'fs', split_axis...  178 us
    all_to_all x1, waiting for transfers between devices, shards(): back = lax.all_to_all(summed, 'fs', split_axis=1, concat_axis=0, tiled=True)  75.6 us
    all_to_all x1, blocking collectives, shards(): lax.all_to_all(down_cast, 'fs', split_axis=0, concat_axis=1, tiled=True)  51.7 us
    unnamed x26, local copies, waits for them, and re-layouts  41.9 us
    all_to_all x1, waiting for transfers between devices, shards(): lax.all_to_all(up_cast, 'fs', split_axis=0, concat_axis=1, tiled=True)  39.5 us
    unnamed x3, other arithmetic  37.4 us
    scatter x1, local copies, waits for them, and re-layouts, shards(): jnp.zeros((experts * capacity, width), jnp.bfloat16).at[target]  33 us
    convert_element_type x1, local copies, waits for them, and re-layouts, shards(): summed = total.astype(jnp.bfloat16)  27 us
  transfers between devices with their start and end apart: 5, of which 3 were waited for; matrix products, arithmetic and copies ran while one was open for 25% of the time, Pallas kernels for 0%

commit v1 on v0

--- a/solution.py
+++ b/solution.py
@@ -7,6 +7,28 @@
 LIMIT = 7.0
 ALPHA = 1.702
 EPS = 1e-06
+
+
+def in_blocks(array, dim, size):
+    before, after = (array.shape[:dim], array.shape[dim + 1 :])
+    return jnp.moveaxis(array.reshape(*before, size, -1, *after), dim, 0)
+
+
+def joined_along(parts, dim):
+    parts = jnp.moveaxis(parts, 0, dim)
+    dims = parts.shape
+    return parts.reshape(*dims[:dim], dims[dim] * dims[dim + 1], *dims[dim + 2 :])
+
+
+def swapped_with_each(x, axis, split_dim, concat_dim):
+    peers, index = (lax.axis_size(axis), lax.axis_index(axis))
+    parts = in_blocks(x, split_dim, peers)
+    finished = [parts[index]]
+    for hop in range(1, peers):
+        sent = parts[index ^ hop]
+        finished.append(lax.ppermute(sent, axis, [(i, i ^ hop) for i in range(peers)]))
+    parts = jnp.stack(finished)[index ^ jnp.arange(peers)]
+    return joined_along(parts, concat_dim)
 
 
 def shards(prompt, routes, route_weight, norm_gain, gate_train, up_train, down_train):
@@ -56,7 +78,7 @@
         ).astype(jnp.bfloat16)
         total = total + part.astype(jnp.float32)
     summed = total.astype(jnp.bfloat16)
-    back = lax.all_to_all(summed, "fs", split_axis=1, concat_axis=0, tiled=True)
+    back = swapped_with_each(summed, "fs", 1, 0)
     picked = back.reshape(experts * capacity, quarter)[target].astype(jnp.float32)
     weighted = picked.reshape(tok_rows, TOP, quarter) * route_weight[:, :, None]
     mixed = jnp.sum(weighted, axis=1).astype(jnp.bfloat16)

time: 605 us -> 565 us (0.934)
  the two profiles are of different devices: /device:TPU:0 before, /device:TPU:9 now
where the time goes in v1:
time: 565 us; the launch traced here: 561 us
  blocking collectives  179 us (32%)
  waiting for transfers between devices  172 us (30%)
  local copies, waits for them, and re-layouts  90.7 us (16%)
  other arithmetic  40.3 us (7%)
  starting transfers between devices  37.1 us (7%)
  matrix products  27.3 us (5%)
  between operations  14.5 us (3%)
    all_to_all x1, blocking collectives, shards(): lax.all_to_all(outbox.reshape(experts, capacity, width), 'fs', split_axis...  179 us
    ppermute x7, waiting for transfers between devices, swapped_with_each(): lax.ppermute(sent, axis, [(i, i ^ hop) for i in range(peers)])  74.5 us
    all_to_all x1, waiting for transfers between devices, shards(): lax.all_to_all(down_cast, 'fs', split_axis=0, concat_axis=1, tiled=True)  45.4 us
    all_to_all x1, waiting for transfers between devices, shards(): lax.all_to_all(up_cast, 'fs', split_axis=0, concat_axis=1, tiled=True)  36 us
    scatter x1, local copies, waits for them, and re-layouts, shards(): jnp.zeros((experts * capacity, width), jnp.bfloat16).at[target]  33.3 us
    unnamed x31, local copies, waits for them, and re-layouts  27.4 us
    unnamed x2, other arithmetic  14.2 us
    all_to_all x1, waiting for transfers between devices, shards(): lax.all_to_all(down_rows, 'tp', split_axis=1, concat_axis=2, tiled=True)  12.8 us
  transfers between devices with their start and end apart: 12, of which 9 were waited for; matrix products, arithmetic and copies ran while one was open for 19% of the time, Pallas kernels for 0%

profile of v1, /device:TPU:9, one launch (start us, length us, event | category | flops | bytes accessed | tf_op | source)
XLA Modules:
  0.0 560.9 jit_solution(3749550151107031715)
XLA Ops:
  7.2 6.8 %multiply_convert_fusion = (bf16[8,256,512]{2,1,0:T(8,128)(2,1)}, bf16[8,256,512]{2,1,0:T(8,128)(2,1)}) fusion(f32[8,256,512]{2,1,0:T(8,128)} %param.12, f32[256]{0:T(256)} %param.10, f32[8,256,512]{2,1,0:T(8,128)} %param.11), kind=kLoop, calls=%fused_computation.8 | loop fusion | flops 4194304 | bytes 12583936 | tf_op jit(solution)/shard_map/convert_element_type | solution.py:36
  14.0 5.7 %all-to-all-start = ((bf16[8,256,512]{2,1,0:T(8,128)(2,1)}), bf16[8,256,512]{2,1,0:T(8,128)(2,1)S(1)}, u32[]{:S(2)}, u32[]{:S(2)}) async-start(bf16[8,256,512]{2,1,0:T(8,128)(2,1)} %get-tuple-element.25), calls=%async_computation | async-start | bytes 4194304 | tf_op jit(solution)/shard_map/all_to_all | solution.py:39
  28.4 33.3 %scatter_custom_fusion = bf16[1920,2048]{1,0:T(8,128)(2,1)} fusion(s32[1536]{0:T(1024)S(1)} %fusion.10, bf16[384,2048]{1,0:T(8,128)(2,1)} %fusion.4, s32[2048]{0:T(1024)S(1)} %pad_clamp_fusion.1, bf16[]{:T(256)} %constant.24.clone.1), kind=kCustom, calls=%fused_computation.5 | custom fusion | bytes 7864832 | tf_op jit(solution)/shard_map/scatter | solution.py:60
  61.8 3.5 all-to-all-done
  65.3 178.7 %all_to_all.63 = bf16[8,240,2048]{2,1,0:T(8,128)(2,1)} all-to-all(bf16[8,240,2048]{2,1,0:T(8,128)(2,1)} %bitcast.85), channel_id=1, replica_groups=mesh['grp'=2,'fs'=8,'tp'=2] {'fs'}, dimensions={0} | all-to-all | bytes 15728640 | tf_op jit(solution)/shard_map/all_to_all | solution.py:61
  244.0 7.2 %all-to-all-start.1 = ((bf16[8,256,512]{2,1,0:T(8,128)(2,1)}), bf16[8,256,512]{2,1,0:T(8,128)(2,1)}, u32[]{:S(2)}, u32[]{:S(2)}) async-start(bf16[8,256,512]{2,1,0:T(8,128)(2,1)} %get-tuple-element.24), calls=%async_computation.1 | async-start | bytes 4194304 | tf_op jit(solution)/shard_map/all_to_all | solution.py:40
  251.2 9.5 %fusion.13 = f32[1920,512]{1,0:T(8,128)} fusion(bf16[1920,2048]{1,0:T(8,128)(2,1)} %bitcast.95, bf16[2048,512]{1,0:T(8,128)(2,1)S(1)} %bitcast.92), kind=kOutput, calls=%fused_computation.61 | convolution fusion | flops 4026531840 | bytes 13893632 | tf_op jit(solution)/shard_map/erd,edf->erf/dot_general | solution.py:64
  260.7 36.0 %all-to-all-done.1 = bf16[8,256,512]{2,1,0:T(8,128)(2,1)} async-done(((bf16[8,256,512]{2,1,0:T(8,128)(2,1)}), bf16[8,256,512]{2,1,0:T(8,128)(2,1)}, u32[]{:S(2)}, u32[]{:S(2)}) %all-to-all-start.1) | async-done | bytes 2097184 | tf_op jit(solution)/shard_map/all_to_all | solution.py:40
  296.7 11.6 %multiply_convert_fusion.2 = bf16[1920,512]{1,0:T(8,128)(2,1)} fusion(f32[1920,512]{1,0:T(8,128)} %fusion.13, bf16[1920,2048]{1,0:T(8,128)(2,1)} %bitcast.96, bf16[2048,512]{1,0:T(8,128)(2,1)} %bitcast.8), kind=kOutput, calls=%fused_computation.10 | convolution fusion | flops 4036362240 | bytes 15859712 | tf_op jit(solution)/shard_map/erd,edf->erf/dot_general | solution.py:65
  308.4 3.8 convert_element_type.60
  312.2 7.4 %all-to-all-start.2 = ((bf16[8,128,1024]{2,1,0:T(8,128)(2,1)}), bf16[8,128,1024]{2,1,0:T(8,128)(2,1)S(1)}, u32[]{:S(2)}, u32[]{:S(2)}) async-start(bf16[8,128,1024]{2,1,0:T(8,128)(2,1)} %convert_element_type.60), calls=%async_computation.2 | async-start | bytes 4194304 | tf_op jit(solution)/shard_map/all_to_all | solution.py:42
  319.7 45.4 %all-to-all-done.2 = bf16[8,128,1024]{2,1,0:T(8,128)(2,1)S(1)} async-done(((bf16[8,128,1024]{2,1,0:T(8,128)(2,1)}), bf16[8,128,1024]{2,1,0:T(8,128)(2,1)S(1)}, u32[]{:S(2)}, u32[]{:S(2)}) %all-to-all-start.2) | async-done | bytes 2097184 | tf_op jit(solution)/shard_map/all_to_all | solution.py:42
  365.1 5.2 copy.39
  370.8 14.1 %reduce.6 = bf16[1024,1024]{1,0:T(8,128)(2,1)} reduce(bf16[1024,1,1024]{2,1,0:T(2,128)(2,1)} %bitcast.86, bf16[]{:T(256)} %broadcast.185), dimensions={1}, to_apply=%bitcast.82.reduce_sub_computation | reduce | bytes 4194306
  384.9 3.8 reshape.245
  388.6 4.9 all-to-all-start.3
  393.6 3.9 fusion.5
  401.9 3.2 collective-permute-start.1
  405.3 12.8 %all-to-all-done.3 = bf16[2,2,262144]{2,1,0:T(2,128)(2,1)} async-done(((bf16[2,2,262144]{2,1,0:T(2,128)(2,1)}), bf16[2,2,262144]{2,1,0:T(2,128)(2,1)}, u32[]{:S(2)}, u32[]{:S(2)}) %all-to-all-start.3) | async-done | bytes 2097184 | tf_op jit(solution)/shard_map/all_to_all | solution.py:43
  418.1 4.5 reshape.246
  428.1 4.0 copy.34
  432.2 3.9 collective-permute-start.2
  444.2 11.2 %collective-permute-done.2 = bf16[1,240,1024]{2,1,0:T(8,128)(2,1)S(1)} collective-permute-done((bf16[1,240,1024]{2,1,0:T(8,128)(2,1)S(1)}, bf16[1,240,1024]{2,1,0:T(8,128)(2,1)S(1)}, u32[]{:S(2)}, u32[]{:S(2)}) %collective-permute-start.2) | collective-permute-done | bytes 491552 | tf_op jit(solution)/shard_map/ppermute | solution.py:29
  456.1 32.0 %collective-permute-done.3 = bf16[1,240,1024]{2,1,0:T(8,128)(2,1)S(1)} collective-permute-done((bf16[1,240,1024]{2,1,0:T(8,128)(2,1)S(1)}, bf16[1,240,1024]{2,1,0:T(8,128)(2,1)S(1)}, u32[]{:S(2)}, u32[]{:S(2)}) %collective-permute-start.3) | collective-permute-done | bytes 491552 | tf_op jit(solution)/shard_map/ppermute | solution.py:29
  489.0 9.8 %collective-permute-done.4 = bf16[1,240,1024]{2,1,0:T(8,128)(2,1)S(1)} collective-permute-done((bf16[1,240,1024]{2,1,0:T(8,128)(2,1)S(1)}, bf16[1,240,1024]{2,1,0:T(8,128)(2,1)S(1)}, u32[]{:S(2)}, u32[]{:S(2)}) %collective-permute-start.4) | collective-permute-done | bytes 491552 | tf_op jit(solution)/shard_map/ppermute | solution.py:29
  499.7 10.8 %collective-permute-done.5 = bf16[1,240,1024]{2,1,0:T(8,128)(2,1)S(1)} collective-permute-done((bf16[1,240,1024]{2,1,0:T(8,128)(2,1)S(1)}, bf16[1,240,1024]{2,1,0:T(8,128)(2,1)S(1)}, u32[]{:S(2)}, u32[]{:S(2)}) %collective-permute-start.5) | collective-permute-done | bytes 491552 | tf_op jit(solution)/shard_map/ppermute | solution.py:29
  511.3 10.6 %collective-permute-done.6 = bf16[1,240,1024]{2,1,0:T(8,128)(2,1)S(1)} collective-permute-done((bf16[1,240,1024]{2,1,0:T(8,128)(2,1)S(1)}, bf16[1,240,1024]{2,1,0:T(8,128)(2,1)S(1)}, u32[]{:S(2)}, u32[]{:S(2)}) %collective-permute-start.6) | collective-permute-done | bytes 491552 | tf_op jit(solution)/shard_map/ppermute | solution.py:29
  522.7 4.8 gather_fusion
  527.5 9.7 %gather_fusion.1 = bf16[1536,1024]{1,0:T(8,128)(2,1)S(1)} fusion(bf16[1920,1024]{1,0:T(8,128)(2,1)} %bitcast.84, s32[2048]{0:T(1024)S(1)} %pad_clamp_fusion), kind=kCustom, calls=%fused_computation.2 | custom fusion | bytes 6297600 | tf_op jit(solution)/shard_map/gather | solution.py:82
  537.2 4.4 reshape.199
  541.6 7.9 %multiply_reduce_fusion = bf16[384,1024]{1,0:T(8,128)(2,1)} fusion(f32[384,4,1024]{2,1,0:T(4,128)} %reshape.199, f32[384,4]{1,0:T(8,128)S(1)} %copy.33), kind=kLoop, calls=%fused_computation.7 | loop fusion | flops 2752512 | bytes 7084032 | tf_op jit(solution)/shard_map/reduce_sum | solution.py:84
  550.8 3.0 copy.50
  (61 shorter events, 32.8 us)
Async XLA Ops:
  14.0 5.7 %copy-start.5 = (s32[384,4]{0,1:T(4,128)S(1)}, s32[384,4]{0,1:T(4,128)}, u32[]{:S(2)}) copy-start(s32[384,4]{0,1:T(4,128)} %param.8) | copy-start | bytes 18436
  14.0 51.3 %all-to-all-start = ((bf16[8,256,512]{2,1,0:T(8,128)(2,1)}), bf16[8,256,512]{2,1,0:T(8,128)(2,1)S(1)}, u32[]{:S(2)}, u32[]{:S(2)}) async-start(bf16[8,256,512]{2,1,0:T(8,128)(2,1)} %get-tuple-element.25), calls=%async_computation | async-start | bytes 4194304 | tf_op jit(solution)/shard_map/all_to_all | solution.py:39
  65.3 185.9 %copy-start = (bf16[8,256,512]{2,1,0:T(8,128)(2,1)}, bf16[8,256,512]{2,1,0:T(8,128)(2,1)S(1)}, u32[]{:S(2)}) copy-start(bf16[8,256,512]{2,1,0:T(8,128)(2,1)S(1)} %all-to-all-done) | copy-start | bytes 6291460
  244.0 52.8 %all-to-all-start.1 = ((bf16[8,256,512]{2,1,0:T(8,128)(2,1)}), bf16[8,256,512]{2,1,0:T(8,128)(2,1)}, u32[]{:S(2)}, u32[]{:S(2)}) async-start(bf16[8,256,512]{2,1,0:T(8,128)(2,1)} %get-tuple-element.24), calls=%async_computation.1 | async-start | bytes 4194304 | tf_op jit(solution)/shard_map/all_to_all | solution.py:40
  251.2 142.4 %all-gather.3.cloned.1.call-start = ((), (), s32[]{:S(2)}) async-start(), calls=%async_computation.5 | async-start | bytes 5898240 | tf_op jit(solution)/shard_map/all_gather | solution.py:72
  312.2 52.9 %all-to-all-start.2 = ((bf16[8,128,1024]{2,1,0:T(8,128)(2,1)}), bf16[8,128,1024]{2,1,0:T(8,128)(2,1)S(1)}, u32[]{:S(2)}, u32[]{:S(2)}) async-start(bf16[8,128,1024]{2,1,0:T(8,128)(2,1)} %convert_element_type.60), calls=%async_computation.2 | async-start | bytes 4194304 | tf_op jit(solution)/shard_map/all_to_all | solution.py:42
  388.6 29.4 %all-to-all-start.3 = ((bf16[2,2,262144]{2,1,0:T(2,128)(2,1)}), bf16[2,2,262144]{2,1,0:T(2,128)(2,1)}, u32[]{:S(2)}, u32[]{:S(2)}) async-start(bf16[2,2,262144]{2,1,0:T(2,128)(2,1)} %reshape.245), calls=%async_computation.3 | async-start | bytes 4194304 | tf_op jit(solution)/shard_map/all_to_all | solution.py:43
  393.6 3.9 copy-start.7
  399.8 5.3 copy-start.6
  401.5 35.8 %collective-permute-start = (bf16[1,240,1024]{2,1,0:T(8,128)(2,1)}, bf16[1,240,1024]{2,1,0:T(8,128)(2,1)}, u32[]{:S(2)}, u32[]{:S(2)}) collective-permute-start(bf16[1,240,1024]{2,1,0:T(8,128)(2,1)} %get-tuple-element.22), channel_id=1, source_target_pairs={{0,2},{2,0},{4,6},{6,4},{8,10},{10,8},{12,14},{14,12},{1,3},{3,1},... | collective-permute-start | bytes 1474568 | tf_op jit(solution)/shard_map/ppermute | solution.py:29
  401.9 38.3 %collective-permute-start.1 = (bf16[1,240,1024]{2,1,0:T(8,128)(2,1)}, bf16[1,240,1024]{2,1,0:T(8,128)(2,1)}, u32[]{:S(2)}, u32[]{:S(2)}) collective-permute-start(bf16[1,240,1024]{2,1,0:T(8,128)(2,1)} %get-tuple-element.21), channel_id=1, source_target_pairs={{0,4},{2,6},{4,0},{6,2},{8,12},{10,14},{12,8},{14,10},{1,5},{3,7},... | collective-permute-start | bytes 1474568 | tf_op jit(solution)/shard_map/ppermute | solution.py:29
  428.1 4.0 copy-start.4
  428.1 7.9 %copy-start.3 = (bf16[1,240,1024]{2,1,0:T(8,128)(2,1)S(1)}, bf16[1,240,1024]{2,1,0:T(8,128)(2,1)}, u32[]{:S(2)}) copy-start(bf16[1,240,1024]{2,1,0:T(8,128)(2,1)} %get-tuple-element.19) | copy-start | bytes 1474564
  428.1 7.9 %copy-start.2 = (bf16[1,240,1024]{2,1,0:T(8,128)(2,1)S(1)}, bf16[1,240,1024]{2,1,0:T(8,128)(2,1)}, u32[]{:S(2)}) copy-start(bf16[1,240,1024]{2,1,0:T(8,128)(2,1)} %get-tuple-element.18) | copy-start | bytes 1474564
  432.2 23.1 %collective-permute-start.2 = (bf16[1,240,1024]{2,1,0:T(8,128)(2,1)S(1)}, bf16[1,240,1024]{2,1,0:T(8,128)(2,1)S(1)}, u32[]{:S(2)}, u32[]{:S(2)}) collective-permute-start(bf16[1,240,1024]{2,1,0:T(8,128)(2,1)S(1)} %copy-done.4), channel_id=1, source_target_pairs={{0,6},{2,4},{4,2},{6,0},{8,14},{10,12},{12,10},{14,8},{1,7},{3,5},... | collective-permute-start | bytes 1474568 | tf_op jit(solution)/shard_map/ppermute | solution.py:29
  436.0 52.1 %collective-permute-start.3 = (bf16[1,240,1024]{2,1,0:T(8,128)(2,1)S(1)}, bf16[1,240,1024]{2,1,0:T(8,128)(2,1)S(1)}, u32[]{:S(2)}, u32[]{:S(2)}) collective-permute-start(bf16[1,240,1024]{2,1,0:T(8,128)(2,1)S(1)} %copy-done.3), channel_id=1, source_target_pairs={{0,8},{2,10},{4,12},{6,14},{8,0},{10,2},{12,4},{14,6},{1,9},{3,11}... | collective-permute-start | bytes 1474568 | tf_op jit(solution)/shard_map/ppermute | solution.py:29
  436.1 62.8 %collective-permute-start.4 = (bf16[1,240,1024]{2,1,0:T(8,128)(2,1)S(1)}, bf16[1,240,1024]{2,1,0:T(8,128)(2,1)S(1)}, u32[]{:S(2)}, u32[]{:S(2)}) collective-permute-start(bf16[1,240,1024]{2,1,0:T(8,128)(2,1)S(1)} %copy-done.2), channel_id=1, source_target_pairs={{0,10},{2,8},{4,14},{6,12},{8,2},{10,0},{12,6},{14,4},{1,11},{3,9}... | collective-permute-start | bytes 1474568 | tf_op jit(solution)/shard_map/ppermute | solution.py:29
  437.3 73.2 %collective-permute-start.5 = (bf16[1,240,1024]{2,1,0:T(8,128)(2,1)S(1)}, bf16[1,240,1024]{2,1,0:T(8,128)(2,1)S(1)}, u32[]{:S(2)}, u32[]{:S(2)}) collective-permute-start(bf16[1,240,1024]{2,1,0:T(8,128)(2,1)S(1)} %get-tuple-element.17), channel_id=1, source_target_pairs={{0,12},{2,14},{4,8},{6,10},{8,4},{10,6},{12,0},{14,2},{1,13},{3,15... | collective-permute-start | bytes 1474568 | tf_op jit(solution)/shard_map/ppermute | solution.py:29
  440.2 81.7 %collective-permute-start.6 = (bf16[1,240,1024]{2,1,0:T(8,128)(2,1)S(1)}, bf16[1,240,1024]{2,1,0:T(8,128)(2,1)S(1)}, u32[]{:S(2)}, u32[]{:S(2)}) collective-permute-start(bf16[1,240,1024]{2,1,0:T(8,128)(2,1)S(1)} %get-tuple-element.16), channel_id=1, source_target_pairs={{0,14},{2,12},{4,10},{6,8},{8,6},{10,4},{12,2},{14,0},{1,15},{3,13... | collective-permute-start | bytes 1474568 | tf_op jit(solution)/shard_map/ppermute | solution.py:29
  541.6 7.9 %copy-start.1 = (bf16[8,256,512]{2,1,0:T(8,128)(2,1)S(1)}, bf16[8,256,512]{2,1,0:T(8,128)(2,1)}, u32[]{:S(2)}) copy-start(bf16[8,256,512]{2,1,0:T(8,128)(2,1)} %copy-done) | copy-start | bytes 6291460
Sparse Core Ops, SparseCore 0:
  308.5 55.3 all-gather.2
